TPU v7x, 256 devices: a whole 4x4x8 slice. The times are simulated.
256 devices in a mesh: sp: 32 (over z, y), tp: 8 (over x, core).
Axes of the slice: x: 4, y: 4, z: 8, core: 2. Of those that a mesh axis runs over, the one named last changes fastest.
Arguments:
- activations: bfloat16 [24576, 2048], P(('sp', 'tp')), may hold values from -6 to 6
- in_gain: float32 [2048], replicated, may hold values from 0.1 to 1.9
- w_pool_in: bfloat16 [2048, 1024], P(None, 'tp'), may hold values from -0.125 to 0.125
- pool_gain: float32 [1024], P('tp'), may hold values from 0.1 to 1.9
- w_qlat: bfloat16 [2048, 768], P(None, 'tp'), may hold values from -0.125 to 0.125
- w_kvlat: bfloat16 [2048, 512], P(None, 'tp'), may hold values from -0.125 to 0.125
- w_krope: bfloat16 [2048, 32], replicated, may hold values from -0.125 to 0.125
- qlat_gain: float32 [768], replicated, may hold values from 0.1 to 1.9
- kvlat_gain: float32 [512], replicated, may hold values from 0.1 to 1.9
- w_qup: bfloat16 [768, 1536], P(None, 'tp'), may hold values from -0.21875 to 0.21875
- w_kup: bfloat16 [512, 1024], P(None, 'tp'), may hold values from -0.25 to 0.25
- w_vup: bfloat16 [512, 1024], P(None, 'tp'), may hold values from -0.25 to 0.25
- qhead_gain: float32 [96], replicated, may hold values from 1.1 to 1.9
- khead_gain: float32 [96], replicated, may hold values from 1.1 to 1.9
- w_out_pool: bfloat16 [1024, 2048], P('tp'), may hold values from -0.1875 to 0.1875
- w_out_attn: bfloat16 [1024, 2048], P('tp'), may hold values from -0.75 to 0.75
Outputs:
- mixed: bfloat16 [24576, 2048], P(('sp', 'tp'))
All inputs are finite; a program needn't handle non-finite values.
Results may differ from a plain program's by a relative error of at most 0.025.
Values may be sent and summed in bfloat16 or wider, within the bound.
No kernel may reach another device: no remote copies, remote signals or barrier semaphores. Data moves between devices by JAX's collectives and lax.ppermute only.
A program may use at most 128 MiB of HBM per device.

v0:
```python
import math
import jax
import jax.numpy as jnp
from jax import lax
from jax.sharding import PartitionSpec as P

GROUP = 256
NOPE = 64
ROPE = 32
VDIM = 64
QLAT = 768
KVLAT = 512
norm_eps = 1e-06
rope_theta = 10000.0
rim_depth = 15
block_rows = 512


def from_behind(block, axis, distance):
    devices = range(lax.axis_size(axis))
    route = [(i - distance, i) for i in devices if i - distance in devices]
    return lax.ppermute(block, axis, route)


def copy_for_each(x, axis):
    copies = jnp.broadcast_to(x, (lax.axis_size(axis), *x.shape))
    return lax.all_to_all(copies, axis, split_axis=0, concat_axis=0, tiled=True)


def of_everyone(x, axis):
    everything = copy_for_each(x, axis)
    return jnp.sum(everything, axis=0)


def together(arrays, axis):
    ends = [0]
    for a in arrays:
        ends.append(ends[-1] + a.size)
    running = of_everyone(jnp.concatenate([a.ravel() for a in arrays]), axis)
    return tuple((running[b:e].reshape(a.shape) for a, b, e in zip(arrays, ends, ends[1:])))


def side_by_side(arrays, axis, dim, along):
    widths = [a.shape[along] for a in arrays]
    both = jnp.concatenate(arrays, axis=along)
    filled = lax.all_gather(both, axis, axis=dim, tiled=True)
    return tuple(jnp.split(filled, [sum(widths[:k]) for k in range(1, len(widths))], axis=along))


def row_norm(source, norm_gain):
    as_float = source.astype(jnp.float32)
    factor = lax.rsqrt(jnp.mean(as_float * as_float, axis=-1, keepdims=True) + norm_eps)
    return as_float * factor * norm_gain


def rotate(head_rows, positions):
    half_rope = ROPE // 2
    frequency = rope_theta ** (-jnp.arange(0, ROPE, 2, dtype=jnp.float32) / ROPE)
    angles = positions.astype(jnp.float32)[:, None] * frequency[None, :]
    cosine = jnp.cos(angles)[:, None, :]
    sine_part = jnp.sin(angles)[:, None, :]
    plain_part = head_rows[..., :NOPE]
    lower_half = head_rows[..., NOPE : NOPE + half_rope]
    upper_half = head_rows[..., NOPE + half_rope :]
    return jnp.concatenate(
        [
            plain_part,
            lower_half * cosine - upper_half * sine_part,
            upper_half * cosine + lower_half * sine_part,
        ],
        axis=-1,
    )


def pool_mix(extended, positions, channel_start):
    row_count = positions.shape[0]
    width = extended.shape[1]
    channel = channel_start + jnp.arange(width, dtype=jnp.int32)
    window = jnp.left_shift(jnp.int32(2), channel // GROUP)
    as_float = extended.astype(jnp.float32)
    window_sum = jnp.zeros((row_count, width), jnp.float32)
    for lag_index in range(rim_depth + 1):
        lagged = as_float[rim_depth - lag_index : rim_depth - lag_index + row_count]
        window_sum = window_sum + jnp.where(lag_index < window[None, :], lagged, 0.0)
    divisor = jnp.minimum(positions[:, None] + 1, window[None, :]).astype(jnp.float32)
    return window_sum / divisor - as_float[rim_depth:]


def make_queries(q_normed, w_qup, norm_gain, positions):
    row_count = q_normed.shape[0]
    head_count = w_qup.shape[1] // (NOPE + ROPE)
    query_raw = jnp.dot(q_normed, w_qup, preferred_element_type=jnp.float32).astype(jnp.bfloat16)
    query_raw = query_raw.reshape(row_count, head_count, NOPE + ROPE)
    return rotate(row_norm(query_raw, norm_gain), positions).astype(jnp.bfloat16)


def plain_parts(kv_rows, w_kup, w_vup):
    key_plain = jnp.dot(kv_rows, w_kup, preferred_element_type=jnp.float32).astype(jnp.bfloat16)
    value_rows = jnp.dot(kv_rows, w_vup, preferred_element_type=jnp.float32).astype(jnp.bfloat16)
    return (key_plain, value_rows)


def finish_keys(key_plain, rope_rows, norm_gain, positions):
    row_count = key_plain.shape[0]
    head_count = key_plain.shape[1] // NOPE
    key_plain = key_plain.reshape(row_count, head_count, NOPE)
    shared = jnp.broadcast_to(rope_rows[:, None, :], (row_count, head_count, ROPE))
    joined = jnp.concatenate([key_plain, shared], axis=-1)
    key_rows = rotate(row_norm(joined, norm_gain), positions).astype(jnp.bfloat16)
    return key_rows.reshape(row_count, head_count * (NOPE + ROPE))


def update(state_pair, queries, query_pos, key_rows, value_rows, key_pos):
    numerator, denominator = state_pair
    head_count = queries.shape[1]
    key_rows = key_rows.reshape(key_rows.shape[0], head_count, NOPE + ROPE)
    value_rows = value_rows.reshape(value_rows.shape[0], head_count, VDIM)
    scores = jnp.einsum("qhd,khd->hqk", queries, key_rows, preferred_element_type=jnp.float32)
    scores = scores * (NOPE + ROPE) ** (-0.5)
    weights = jnp.where(key_pos[None, None, :] <= query_pos[None, :, None], jnp.exp(scores), 0.0)
    denominator = denominator + jnp.sum(weights, axis=-1)
    numerator = numerator + jnp.einsum(
        "hqk,khd->qhd", weights.astype(jnp.bfloat16), value_rows, preferred_element_type=jnp.float32
    )
    return (numerator, denominator)


def sweep(state_pair, pieces, expand, queries, query_pos):
    shard_rows = queries.shape[0]
    piece_rows = pieces[0].shape[0]
    block_size = shard_rows * math.gcd(piece_rows // shard_rows, max(1, block_rows // shard_rows))

    def advance(block_index, current):
        offset = block_index * block_size

        def accumulate(inner):
            chosen = tuple(
                (lax.dynamic_slice_in_dim(member, offset, block_size, 0) for member in pieces)
            )
            key_pos = offset + jnp.arange(block_size, dtype=jnp.int32)
            key_rows, value_rows = expand(chosen, key_pos)
            return update(inner, queries, query_pos, key_rows, value_rows, key_pos)

        def unchanged(inner):
            return inner

        return lax.cond(offset <= query_pos[-1], accumulate, unchanged, current)

    return lax.fori_loop(0, piece_rows // block_size, advance, state_pair)


def local(
    activations,
    in_gain,
    w_pool_in,
    pool_gain,
    w_qlat,
    w_kvlat,
    w_krope,
    qlat_gain,
    kvlat_gain,
    w_qup,
    w_kup,
    w_vup,
    qhead_gain,
    khead_gain,
    w_out_pool,
    w_out_attn,
):
    own_input = lax.all_gather(activations, "tp", axis=0, tiled=True)
    row_count = own_input.shape[0]
    positions = lax.axis_index("sp") * row_count + jnp.arange(row_count, dtype=jnp.int32)
    normed = row_norm(own_input, in_gain).astype(jnp.bfloat16)
    pool_in = jnp.dot(normed, w_pool_in, preferred_element_type=jnp.float32).astype(jnp.bfloat16)
    prev_rows = from_behind(pool_in[row_count - rim_depth :], "sp", 1)
    extended = jnp.concatenate([prev_rows, pool_in], axis=0)
    channel_start = lax.axis_index("tp") * pool_in.shape[1]
    pool_out = (pool_mix(extended, positions, channel_start) * pool_gain).astype(jnp.bfloat16)
    q_part = jnp.dot(normed, w_qlat, preferred_element_type=jnp.float32).astype(jnp.bfloat16)
    kv_part = jnp.dot(normed, w_kvlat, preferred_element_type=jnp.float32).astype(jnp.bfloat16)
    rope_key = jnp.dot(normed, w_krope, preferred_element_type=jnp.float32).astype(jnp.bfloat16)
    tp_index = lax.axis_index("tp")
    q_width = q_part.shape[1]
    kv_width = kv_part.shape[1]
    q_float = q_part.astype(jnp.float32)
    kv_float = kv_part.astype(jnp.float32)
    q_squares, kv_squares = together(
        (jnp.sum(q_float * q_float, axis=1), jnp.sum(kv_float * kv_float, axis=1)), "tp"
    )
    q_gain = lax.dynamic_slice_in_dim(qlat_gain, tp_index * q_width, q_width)
    kv_gain = lax.dynamic_slice_in_dim(kvlat_gain, tp_index * kv_width, kv_width)
    q_scaled = q_float * lax.rsqrt(q_squares / QLAT + norm_eps)[:, None] * q_gain
    kv_scaled = kv_float * lax.rsqrt(kv_squares / KVLAT + norm_eps)[:, None] * kv_gain
    q_normed, kv_normed = (
        lax.all_gather(q_scaled.astype(jnp.bfloat16), "tp", axis=1, tiled=True),
        lax.all_gather(kv_scaled.astype(jnp.bfloat16), "tp", axis=1, tiled=True),
    )
    queries = make_queries(q_normed, w_qup, qhead_gain, positions)
    head_count = queries.shape[1]
    start_pair = (
        jnp.zeros((row_count, head_count, VDIM), jnp.float32),
        jnp.zeros((head_count, row_count), jnp.float32),
    )
    key_plain, value_rows = plain_parts(kv_normed, w_kup, w_vup)

    def expand_plain(chosen, key_pos):
        return (finish_keys(chosen[0], chosen[2], khead_gain, key_pos), chosen[1])

    numerator, denominator = sweep(
        start_pair,
        side_by_side((key_plain, value_rows, rope_key), "sp", 0, 1),
        expand_plain,
        queries,
        positions,
    )
    attended = (numerator / jnp.transpose(denominator)[:, :, None]).astype(jnp.bfloat16)
    attended = attended.reshape(row_count, head_count * VDIM)
    term = jnp.dot(pool_out, w_out_pool, preferred_element_type=jnp.float32)
    return lax.psum_scatter(
        (term + jnp.dot(attended, w_out_attn, preferred_element_type=jnp.float32)).astype(
            jnp.bfloat16
        ),
        "tp",
        scatter_dimension=0,
        tiled=True,
    )


def solution(mesh):
    placed = (
        P(("sp", "tp"), None),
        P(),
        P(None, "tp"),
        P("tp"),
        P(None, "tp"),
        P(None, "tp"),
        P(),
        P(),
        P(),
        P(None, "tp"),
        P(None, "tp"),
        P(None, "tp"),
        P(),
        P(),
        P("tp", None),
        P("tp", None),
    )
    return jax.shard_map(
        local, mesh=mesh, in_specs=placed, out_specs=P(("sp", "tp"), None), check_vma=False
    )
```

profile of v0, /device:TPU:8, one launch (start us, length us, event | category | flops | bytes accessed | tf_op | source)
XLA Modules:
  0.0 467.7 jit_solution(14622654200361501160)
XLA Ops:
  6.5 0.7 all-gather.4.cloned.1.call-update
  7.3 35.0 %all-gather.4.cloned.1.call-done = bf16[768,2048]{1,0:T(8,128)(2,1)} async-done(((bf16[96,2048]{1,0:T(8,128)(2,1)}), bf16[768,2048]{1,0:T(8,128)(2,1)}) %all-gather.4.cloned.1.call-update) | async-done | bytes 3145744 | tf_op jit(solution)/shard_map/all_gather | solution.py:170
  42.3 2.7 fusion.23
  45.1 1.5 fusion.25
  46.7 1.1 multiply_reduce_fusion.1
  47.8 1.1 multiply_reduce_fusion
  49.6 3.3 all-to-all-start
  53.0 0.8 dynamic_slice.16
  53.8 4.6 all-to-all-done
  58.5 0.7 multiply_convert_fusion
  59.3 0.8 dynamic_slice.15
  60.1 3.0 convolution_convert_fusion.6
  63.1 14.2 %all_gather.13 = bf16[768,512]{0,1:T(8,128)(2,1)S(1)} all-gather(bf16[768,64]{0,1:T(8,128)(2,1)S(1)} %multiply_convert_fusion.1), channel_id=1, replica_groups=mesh['sp'=32,'tp'=8] {'tp'}, dimensions={1}, use_global_device_ids=true | all-gather | bytes 884736 | tf_op jit(solution)/shard_map/all_gather | solution.py:196
  78.0 0.8 pad_maximum_fusion.1
  79.4 2.9 convolution_convert_fusion.1
  82.3 3.6 collective-permute-start
  85.9 1.9 collective-permute-done
  87.9 4.2 fusion.49
  92.1 1.7 convolution_convert_fusion
  94.1 119.7 %all-gather.6.cloned.1.call-done = bf16[24576,288]{0,1:T(8,128)(2,1)} async-done(((bf16[768,288]{0,1:T(8,128)(2,1)}), bf16[24576,288]{0,1:T(8,128)(2,1)}) %all-gather.6.cloned.1.call-update) | async-done | bytes 14155792 | tf_op jit(solution)/shard_map/all_gather | solution.py:46
  213.8 1.5 split.14
  215.3 10.4 %fusion.79 = (bf16[24576,128]{0,1:T(8,128)(2,1)}, bf16[24576,128]{0,1:T(8,128)(2,1)}) fusion(bf16[24576,288]{0,1:T(8,128)(2,1)} %all-gather.6.cloned.1.call-done), kind=kLoop, calls=%fused_computation.156 | loop fusion | bytes 25165824 | tf_op jit(solution)/shard_map/split | solution.py:47
  225.7 54.0 %while.15 = (s32[]{:T(128)}, f32[768,2,64]{0,2,1:T(8,128)S(1)}, f32[2,768]{1,0:T(2,128)S(1)}, s32[768]{0:T(1024)S(1)}, bf16[24576,128]{0,1:T(8,128)(2,1)}, /*ind...) while((s32[]{:T(128)}, f32[768,2,64]{0,2,1:T(8,128)S(1)}, ...), condition=%wide.region_10.11_spmd, body=%wide.region_5.10_spmd.sunk | while | flops 388119616 | bytes 15941421 | solution.py:149
  225.7 0.7 slice.283
  227.1 4.7 %conditional.2 = ((f32[768,2,64]{0,2,1:T(8,128)S(1)}, f32[2,768]{1,0:T(2,128)S(1)})) conditional(s32[]{:T(128)} %convert_element_type.159, (f32[768,2,64]{0,2,1:T(8,128)S(1)}, f32[2,768]{1,0:T(2,128)S(1)}) %tuple.56, (s32[]{:T(128)}, bf16[24576,128]{0,1:T(8,128)(2,1)}, s32[768]{0:T(1024)S(1)}, bf16[24576,128]{0,1:T(8,128)(2,1)}, ...), branch_computations={%region_6.6_spmd, %region_7.9_spmd} | conditional | flops 388119616 | bytes 15941190 | solution.py:147
  227.2 1.1 constant_dynamic-slice_fusion.1
  229.2 1.4 fusion
  230.5 1.2 fusion.8
  231.8 0.7 slice.283
  233.2 4.7 %conditional.2 = ((f32[768,2,64]{0,2,1:T(8,128)S(1)}, f32[2,768]{1,0:T(2,128)S(1)})) conditional(s32[]{:T(128)} %convert_element_type.159, (f32[768,2,64]{0,2,1:T(8,128)S(1)}, f32[2,768]{1,0:T(2,128)S(1)}) %tuple.56, (s32[]{:T(128)}, bf16[24576,128]{0,1:T(8,128)(2,1)}, s32[768]{0:T(1024)S(1)}, bf16[24576,128]{0,1:T(8,128)(2,1)}, ...), branch_computations={%region_6.6_spmd, %region_7.9_spmd} | conditional | flops 388119616 | bytes 15941190 | solution.py:147
  233.3 1.1 constant_dynamic-slice_fusion.1
  235.3 1.4 fusion
  236.6 1.2 fusion.8
  237.9 0.7 slice.283
  239.3 0.7 slice.283
  240.7 0.7 slice.283
  242.1 0.7 slice.283
  243.5 0.7 slice.283
  244.9 0.7 slice.283
  246.3 0.7 slice.283
  247.7 0.7 slice.283
  249.1 0.7 slice.283
  251.9 0.7 slice.283
  253.2 0.7 slice.283
  254.6 0.7 slice.283
  256.0 0.7 slice.283
  279.8 5.4 %add_convert_fusion.1 = bf16[768,2048]{1,0:T(8,128)(2,1)} fusion(f32[768,2048]{1,0:T(8,128)} %fusion.49, bf16[768,128]{0,1:T(8,128)(2,1)S(1)} %bitcast.48, bf16[128,2048]{1,0:T(8,128)(2,1)S(1)} %copy-done.3), kind=kOutput, calls=%fused_computation.39 | convolution fusion | flops 405798912 | bytes 10158080 | tf_op jit(solution)/shard_map/dot_general | solution.py:220
  285.2 175.9 %reduce-scatter.2.cloned.1.call-done = bf16[96,2048]{1,0:T(8,128)(2,1)} async-done(((bf16[768,2048]{1,0:T(8,128)(2,1)}), bf16[96,2048]{1,0:T(8,128)(2,1)}) %reduce-scatter.2.cloned.1.call-update) | async-done | bytes 393232 | tf_op jit(solution)/shard_map/reduce_scatter | solution.py:219
  (140 shorter events, 16.0 us)
Async XLA Ops:
  6.5 81.3 %copy-start = (bf16[128,2048]{1,0:T(8,128)(2,1)S(1)}, bf16[128,2048]{1,0:T(8,128)(2,1)}, u32[]{:S(2)}) copy-start(bf16[128,2048]{1,0:T(8,128)(2,1)} %param.34) | copy-start | bytes 1572868
  6.5 35.8 %all-gather.4.cloned.1.call-start = ((), (), s32[]{:S(2)}) async-start(), calls=%async_computation.2 | async-start | bytes 3538944 | tf_op jit(solution)/shard_map/all_gather | solution.py:170
  42.3 2.8 copy-start.2
  42.3 4.4 copy-start.6
  45.1 2.7 copy-start.4
  46.7 2.2 copy-start.1
  46.7 13.4 %copy-start.7 = (bf16[2048,32]{0,1:T(8,128)(2,1)S(1)}, bf16[2048,32]{0,1:T(8,128)(2,1)}, u32[]{:S(2)}) copy-start(bf16[2048,32]{0,1:T(8,128)(2,1)} %param.26) | copy-start | bytes 393220
  48.9 28.4 %copy-start.8 = (bf16[512,128]{1,0:T(8,128)(2,1)S(1)}, bf16[512,128]{1,0:T(8,128)(2,1)}, u32[]{:S(2)}) copy-start(bf16[512,128]{1,0:T(8,128)(2,1)} %param.31) | copy-start | bytes 393220
  48.9 28.7 %copy-start.9 = (bf16[512,128]{1,0:T(8,128)(2,1)S(1)}, bf16[512,128]{1,0:T(8,128)(2,1)}, u32[]{:S(2)}) copy-start(bf16[512,128]{1,0:T(8,128)(2,1)} %param.30) | copy-start | bytes 393220
  49.6 8.8 %all-to-all-start = ((f32[8,1,1536]{2,1,0:T(1,128)}), f32[8,1,1536]{2,1,0:T(1,128)S(1)}, u32[]{:S(2)}, u32[]{:S(2)}) async-start(f32[8,1,1536]{2,1,0:T(1,128)} %broadcast_in_dim.188), calls=%async_computation | async-start | bytes 98304 | tf_op jit(solution)/shard_map/all_to_all | solution.py:27
  53.0 39.1 %all-gather.8.cloned.1.call-start = ((), (), s32[]{:S(2)}) async-start(), calls=%async_computation.4 | async-start | bytes 1327104 | tf_op jit(solution)/shard_map/all_gather | solution.py:195
  59.3 154.5 %all-gather.6.cloned.1.call-start = ((), (), s32[]{:S(2)}) async-start(), calls=%async_computation.3 | async-start | bytes 14598144 | tf_op jit(solution)/shard_map/all_gather | solution.py:46
  60.1 19.3 %copy-start.12 = (bf16[2048,128]{1,0:T(8,128)(2,1)S(1)}, bf16[2048,128]{1,0:T(8,128)(2,1)}, u32[]{:S(2)}) copy-start(bf16[2048,128]{1,0:T(8,128)(2,1)} %param.22) | copy-start | bytes 1572868
  77.4 10.5 %copy-start.13 = (f32[128]{0:T(128)S(1)}, f32[128]{0:T(128)}, u32[]{:S(2)}) copy-start(f32[128]{0:T(128)} %param.23) | copy-start | bytes 1540
  78.9 382.3 %reduce-scatter.2.cloned.1.call-start = ((), (), s32[]{:S(2)}) async-start(), calls=%async_computation.5 | async-start | bytes 3538944 | tf_op jit(solution)/shard_map/reduce_scatter | solution.py:219
  82.3 5.5 %collective-permute-start = (bf16[15,128]{1,0:T(8,128)(2,1)S(1)}, bf16[15,128]{1,0:T(8,128)(2,1)S(1)}, u32[]{:S(2)}, u32[]{:S(2)}) collective-permute-start(bf16[15,128]{1,0:T(8,128)(2,1)S(1)} %slice.110), channel_id=1, source_target_pairs={{0,8},{8,16},{16,24},{24,32},{32,40},{40,48},{48,56},{56,64},{64,7... | collective-permute-start | bytes 11528 | tf_op jit(solution)/shard_map/ppermute | solution.py:22
  87.9 4.2 copy-start.5
  87.9 6.0 %copy-start.11 = (f32[96]{0:T(128)S(1)}, f32[96]{0:T(128)}, u32[]{:S(2)}) copy-start(f32[96]{0:T(128)} %param.32) | copy-start | bytes 1156
  215.3 10.4 %copy-start.10 = (f32[96]{0:T(128)S(1)}, f32[96]{0:T(128)}, u32[]{:S(2)}) copy-start(f32[96]{0:T(128)} %param.33) | copy-start | bytes 1156
  225.7 54.0 %copy-start.3 = (bf16[128,2048]{1,0:T(8,128)(2,1)S(1)}, bf16[128,2048]{1,0:T(8,128)(2,1)}, u32[]{:S(2)}) copy-start(bf16[128,2048]{1,0:T(8,128)(2,1)} %param.35) | copy-start | bytes 1572868
Sparse Core Ops, SparseCore 0:
  9.2 33.0 all-gather.3
  59.4 26.1 all-gather.7
  88.2 125.5 all-gather.5
  285.3 175.7 reduce-scatter.1
where the time goes:
time: 469 us; the launch traced here: 468 us
  waiting for transfers between devices  338 us (72%)
  local copies, waits for them, and re-layouts  37.6 us (8%)
  matrix products  25.2 us (5%)
  loops' own time  23.6 us (5%)
  blocking collectives  14.2 us (3%)
  between operations  13.5 us (3%)
  other arithmetic  8.52 us (2%)
  starting transfers between devices  7.03 us (1%)
    reduce_scatter x1, waiting for transfers between devices, local(): lax.psum_scatter((term + jnp.dot(attended, w_out_attn, preferred_element_...  176 us
    all_gather x1, waiting for transfers between devices, side_by_side(): filled = lax.all_gather(both, axis, axis=dim, tiled=True)  120 us
    all_gather x1, waiting for transfers between devices, local(): own_input = lax.all_gather(activations, 'tp', axis=0, tiled=True)  35 us
    another operation x1, loops' own time, sweep(): return lax.fori_loop(0, piece_rows // block_size, advance, state_pair)  23.1 us
    slice x32, local copies, waits for them, and re-layouts, advance(): return lax.cond(offset <= query_pos[-1], accumulate, unchanged, current)  21.2 us
    all_gather x1, blocking collectives, local(): lax.all_gather(kv_scaled.astype(jnp.bfloat16), 'tp', axis=1, tiled=True)  14.2 us
    split x2, local copies, waits for them, and re-layouts, side_by_side(): jnp.split(filled, [sum(widths[:k]) for k in range(1, len(widths))], axis=...  11.9 us
  transfers between devices with their start and end apart: 6, of which 5 were waited for; matrix products, arithmetic and copies ran while one was open for 3% of the time, Pallas kernels for 0%

commit v1 on v0

--- a/solution.py
+++ b/solution.py
@@ -167,7 +167,9 @@
     w_out_pool,
     w_out_attn,
 ):
-    own_input = lax.all_gather(activations, "tp", axis=0, tiled=True)
+    own_input = jnp.concatenate(
+        lax.all_to_all(jnp.stack([activations] * lax.axis_size("tp")), "tp", 0, 0), axis=0
+    )
     row_count = own_input.shape[0]
     positions = lax.axis_index("sp") * row_count + jnp.arange(row_count, dtype=jnp.int32)
     normed = row_norm(own_input, in_gain).astype(jnp.bfloat16)

time: 469 us -> 473 us (level)
  blocking collectives: 14.2 us -> 55.9 us
  waiting for transfers between devices: 338 us -> 304 us
    all_to_all x0 -> x1, blocking collectives: none -> 42.5 us  [local(): lax.all_to_all(jnp.stack([activations] * lax.axis_size('tp')), 'tp', 0, 0)]
    all_gather x1 -> x0, waiting for transfers between devices: 35 us -> none  [local(): own_input = lax.all_gather(activations, 'tp', axis=0, tiled=True)]
  transfers between devices with their start and end apart: 6 -> 5, of which waited for: 5 -> 4; matrix products, arithmetic and copies ran while one was open for 3% -> 3% of each run, Pallas kernels for 0% -> 0%
where the time goes in v1:
time: 473 us; the launch traced here: 472 us
  waiting for transfers between devices  304 us (64%)
  blocking collectives  55.9 us (12%)
  local copies, waits for them, and re-layouts  38.3 us (8%)
  matrix products  25.2 us (5%)
  loops' own time  19.8 us (4%)
  between operations  13.5 us (3%)
  other arithmetic  7.69 us (2%)
  starting transfers between devices  7.14 us (2%)
    reduce_scatter x1, waiting for transfers between devices, local(): lax.psum_scatter((term + jnp.dot(attended, w_out_attn, preferred_element_...  176 us
    all_gather x1, waiting for transfers between devices, side_by_side(): filled = lax.all_gather(both, axis, axis=dim, tiled=True)  122 us
    all_to_all x1, blocking collectives, local(): lax.all_to_all(jnp.stack([activations] * lax.axis_size('tp')), 'tp', 0, 0)  42.5 us
    another operation x1, loops' own time, sweep(): return lax.fori_loop(0, piece_rows // block_size, advance, state_pair)  19.3 us
    slice x32, local copies, waits for them, and re-layouts, advance(): return lax.cond(offset <= query_pos[-1], accumulate, unchanged, current)  18.7 us
    all_gather x1, blocking collectives, local(): lax.all_gather(kv_scaled.astype(jnp.bfloat16), 'tp', axis=1, tiled=True)  13.4 us
    split x2, local copies, waits for them, and re-layouts, side_by_side(): jnp.split(filled, [sum(widths[:k]) for k in range(1, len(widths))], axis=...  11.9 us
  transfers between devices with their start and end apart: 5, of which 4 were waited for; matrix products, arithmetic and copies ran while one was open for 3% of the time, Pallas kernels for 0%

profile of v1, /device:TPU:8, one launch (start us, length us, event | category | flops | bytes accessed | tf_op | source)
XLA Modules:
  0.0 472.0 jit_solution(7645813855571118134)
XLA Ops:
  6.5 1.4 stack.2
  8.0 42.5 %all_to_all.11 = bf16[8,96,2048]{2,1,0:T(8,128)(2,1)S(1)} all-to-all(bf16[8,96,2048]{2,1,0:T(8,128)(2,1)S(1)} %stack.2), channel_id=1, replica_groups=mesh['sp'=32,'tp'=8] {'tp'}, dimensions={0} | all-to-all | bytes 6291456 | tf_op jit(solution)/shard_map/all_to_all | solution.py:171
  50.5 1.6 copy-done.2
  52.2 0.7 multiply_reduce_fusion
  53.0 2.7 fusion.24
  55.7 1.1 multiply_reduce_fusion.2
  56.8 1.1 multiply_reduce_fusion.1
  58.0 0.6 broadcast_in_dim.188
  58.7 3.3 all-to-all-start.1
  62.1 0.8 dynamic_slice.16
  62.8 4.6 all-to-all-done.1
  67.5 0.7 multiply_convert_fusion
  68.3 0.8 dynamic_slice.15
  69.1 3.0 convolution_convert_fusion.6
  72.2 13.4 %all_gather.9 = bf16[768,512]{0,1:T(8,128)(2,1)S(1)} all-gather(bf16[768,64]{0,1:T(8,128)(2,1)S(1)} %multiply_convert_fusion.1), channel_id=1, replica_groups=mesh['sp'=32,'tp'=8] {'tp'}, dimensions={1}, use_global_device_ids=true | all-gather | bytes 884736 | tf_op jit(solution)/shard_map/all_gather | solution.py:198
  86.2 0.8 pad_maximum_fusion.1
  87.6 2.9 convolution_convert_fusion.1
  90.5 3.7 collective-permute-start
  94.2 1.8 collective-permute-done
  96.1 4.2 fusion.48
  100.3 1.7 convolution_convert_fusion
  102.3 122.1 %all-gather.3.cloned.1.call-done = bf16[24576,288]{0,1:T(8,128)(2,1)} async-done(((bf16[768,288]{0,1:T(8,128)(2,1)}), bf16[24576,288]{0,1:T(8,128)(2,1)}) %all-gather.3.cloned.1.call-update) | async-done | bytes 14155792 | tf_op jit(solution)/shard_map/all_gather | solution.py:46
  224.3 1.5 split.14
  225.9 10.4 %fusion.78 = (bf16[24576,128]{0,1:T(8,128)(2,1)}, bf16[24576,128]{0,1:T(8,128)(2,1)}) fusion(bf16[24576,288]{0,1:T(8,128)(2,1)} %all-gather.3.cloned.1.call-done), kind=kLoop, calls=%fused_computation.155 | loop fusion | bytes 25165824 | tf_op jit(solution)/shard_map/split | solution.py:47
  236.3 47.8 %while.15 = (s32[]{:T(128)}, f32[768,2,64]{0,2,1:T(8,128)S(1)}, f32[2,768]{1,0:T(2,128)S(1)}, s32[768]{0:T(1024)S(1)}, bf16[24576,128]{0,1:T(8,128)(2,1)}, /*ind...) while((s32[]{:T(128)}, f32[768,2,64]{0,2,1:T(8,128)S(1)}, ...), condition=%wide.region_10.11_spmd, body=%wide.region_5.10_spmd.sunk | while | flops 388119616 | bytes 15941421 | solution.py:149
  236.4 0.6 slice.283
  237.5 4.7 %conditional.2 = ((f32[768,2,64]{0,2,1:T(8,128)S(1)}, f32[2,768]{1,0:T(2,128)S(1)})) conditional(s32[]{:T(128)} %convert_element_type.162, (f32[768,2,64]{0,2,1:T(8,128)S(1)}, f32[2,768]{1,0:T(2,128)S(1)}) %tuple.56, (s32[]{:T(128)}, bf16[24576,128]{0,1:T(8,128)(2,1)}, s32[768]{0:T(1024)S(1)}, bf16[24576,128]{0,1:T(8,128)(2,1)}, ...), branch_computations={%region_6.6_spmd, %region_7.9_spmd} | conditional | flops 388119616 | bytes 15941190 | solution.py:147
  237.6 1.1 constant_dynamic-slice_fusion.1
  239.6 1.4 fusion
  241.0 1.2 fusion.8
  242.3 0.6 slice.283
  243.4 4.7 conditional.2
  243.5 1.1 constant_dynamic-slice_fusion.1
  245.5 1.4 fusion
  246.9 1.2 fusion.8
  248.2 0.6 slice.283
  250.6 0.6 slice.283
  251.8 0.6 slice.283
  253.0 0.6 slice.283
  254.2 0.6 slice.283
  255.4 0.6 slice.283
  256.6 0.6 slice.283
  257.8 0.6 slice.283
  260.2 0.6 slice.283
  261.4 0.6 slice.283
  262.6 0.6 slice.283
  284.2 5.4 %add_convert_fusion.1 = bf16[768,2048]{1,0:T(8,128)(2,1)} fusion(f32[768,2048]{1,0:T(8,128)} %fusion.48, bf16[768,128]{0,1:T(8,128)(2,1)S(1)} %bitcast.54, bf16[128,2048]{1,0:T(8,128)(2,1)S(1)} %copy-done.3), kind=kOutput, calls=%fused_computation.37 | convolution fusion | flops 405798912 | bytes 10158080 | tf_op jit(solution)/shard_map/dot_general | solution.py:222
  289.6 175.9 %reduce-scatter.2.cloned.1.call-done = bf16[96,2048]{1,0:T(8,128)(2,1)} async-done(((bf16[768,2048]{1,0:T(8,128)(2,1)}), bf16[96,2048]{1,0:T(8,128)(2,1)}) %reduce-scatter.2.cloned.1.call-update) | async-done | bytes 393232 | tf_op jit(solution)/shard_map/reduce_scatter | solution.py:221
  (142 shorter events, 15.2 us)
Async XLA Ops:
  6.5 89.5 %copy-start = (bf16[128,2048]{1,0:T(8,128)(2,1)S(1)}, bf16[128,2048]{1,0:T(8,128)(2,1)}, u32[]{:S(2)}) copy-start(bf16[128,2048]{1,0:T(8,128)(2,1)} %param.34) | copy-start | bytes 1572868
  8.0 45.0 %copy-start.11 = (f32[2048]{0:T(1024)S(1)}, f32[2048]{0:T(1024)}, u32[]{:S(2)}) copy-start(f32[2048]{0:T(1024)} %param.21) | copy-start | bytes 24580
  50.5 1.6 copy-start.2
  52.2 3.5 copy-start.6
  53.0 3.9 copy-start.4
  55.7 2.3 copy-start.1
  55.7 13.4 %copy-start.7 = (bf16[2048,32]{0,1:T(8,128)(2,1)S(1)}, bf16[2048,32]{0,1:T(8,128)(2,1)}, u32[]{:S(2)}) copy-start(bf16[2048,32]{0,1:T(8,128)(2,1)} %param.26) | copy-start | bytes 393220
  58.0 27.6 %copy-start.8 = (bf16[512,128]{1,0:T(8,128)(2,1)S(1)}, bf16[512,128]{1,0:T(8,128)(2,1)}, u32[]{:S(2)}) copy-start(bf16[512,128]{1,0:T(8,128)(2,1)} %param.31) | copy-start | bytes 393220
  58.0 27.9 %copy-start.9 = (bf16[512,128]{1,0:T(8,128)(2,1)S(1)}, bf16[512,128]{1,0:T(8,128)(2,1)}, u32[]{:S(2)}) copy-start(bf16[512,128]{1,0:T(8,128)(2,1)} %param.30) | copy-start | bytes 393220
  58.7 8.8 %all-to-all-start.1 = ((f32[8,1,1536]{2,1,0:T(1,128)}), f32[8,1,1536]{2,1,0:T(1,128)S(1)}, u32[]{:S(2)}, u32[]{:S(2)}) async-start(f32[8,1,1536]{2,1,0:T(1,128)} %broadcast_in_dim.188), calls=%async_computation.1 | async-start | bytes 98304 | tf_op jit(solution)/shard_map/all_to_all | solution.py:27
  62.0 38.3 %all-gather.5.cloned.1.call-start = ((), (), s32[]{:S(2)}) async-start(), calls=%async_computation.4 | async-start | bytes 1327104 | tf_op jit(solution)/shard_map/all_gather | solution.py:197
  68.3 156.0 %all-gather.3.cloned.1.call-start = ((), (), s32[]{:S(2)}) async-start(), calls=%async_computation.3 | async-start | bytes 14598144 | tf_op jit(solution)/shard_map/all_gather | solution.py:46
  69.1 18.5 %copy-start.13 = (bf16[2048,128]{1,0:T(8,128)(2,1)S(1)}, bf16[2048,128]{1,0:T(8,128)(2,1)}, u32[]{:S(2)}) copy-start(bf16[2048,128]{1,0:T(8,128)(2,1)} %param.22) | copy-start | bytes 1572868
  85.6 10.5 %copy-start.14 = (f32[128]{0:T(128)S(1)}, f32[128]{0:T(128)}, u32[]{:S(2)}) copy-start(f32[128]{0:T(128)} %param.23) | copy-start | bytes 1540
  87.1 378.4 %reduce-scatter.2.cloned.1.call-start = ((), (), s32[]{:S(2)}) async-start(), calls=%async_computation.5 | async-start | bytes 3538944 | tf_op jit(solution)/shard_map/reduce_scatter | solution.py:221
  90.5 5.5 %collective-permute-start = (bf16[15,128]{1,0:T(8,128)(2,1)S(1)}, bf16[15,128]{1,0:T(8,128)(2,1)S(1)}, u32[]{:S(2)}, u32[]{:S(2)}) collective-permute-start(bf16[15,128]{1,0:T(8,128)(2,1)S(1)} %slice.110), channel_id=1, source_target_pairs={{0,8},{8,16},{16,24},{24,32},{32,40},{40,48},{48,56},{56,64},{64,7... | collective-permute-start | bytes 11528 | tf_op jit(solution)/shard_map/ppermute | solution.py:22
  96.0 4.2 copy-start.5
  96.1 6.0 %copy-start.12 = (f32[96]{0:T(128)S(1)}, f32[96]{0:T(128)}, u32[]{:S(2)}) copy-start(f32[96]{0:T(128)} %param.32) | copy-start | bytes 1156
  225.9 10.5 %copy-start.10 = (f32[96]{0:T(128)S(1)}, f32[96]{0:T(128)}, u32[]{:S(2)}) copy-start(f32[96]{0:T(128)} %param.33) | copy-start | bytes 1156
  236.3 47.8 %copy-start.3 = (bf16[128,2048]{1,0:T(8,128)(2,1)S(1)}, bf16[128,2048]{1,0:T(8,128)(2,1)}, u32[]{:S(2)}) copy-start(bf16[128,2048]{1,0:T(8,128)(2,1)} %param.35) | copy-start | bytes 1572868
Sparse Core Ops, SparseCore 0:
  68.4 26.9 all-gather.4
  98.1 126.2 all-gather.2
  289.8 175.7 reduce-scatter.1
